TPU v7x, 32 devices: a whole 2x2x4 slice. The times are simulated.
32 devices in a mesh: fs: 16 (over z, y, x), tp: 2 (over core).
Axes of the slice: x: 2, y: 2, z: 4, core: 2. Of those that a mesh axis runs over, the one named last changes fastest.
Arguments:
- tokens: bfloat16 [8192, 2048], P('fs'), may hold values from -6 to 6
- norm_gain: float32 [2048], P('fs'), may hold values from 0.1 to 1.9
- w_gate: float32 [16, 2048, 512], P(None, 'fs', 'tp'), may hold values from -0.125 to 0.125
- w_up: float32 [16, 2048, 512], P(None, 'fs', 'tp'), may hold values from -0.125 to 0.125
- w_down: float32 [16, 2048, 512], P(None, 'fs', 'tp'), may hold values from -0.25 to 0.25
- route_expert: int32 [8192, 2], P('fs'), may hold values from 0 to 15, as said below
- group_prob: float32 [8192], P('fs'), may hold values from 0.25 to 1
- pair_logit: float32 [8192, 2], P('fs'), may hold values from -6 to 6
Outputs:
- new_gate: bfloat16 [16, 2048, 512], P('fs', None, 'tp')
- new_up: bfloat16 [16, 2048, 512], P('fs', None, 'tp')
- new_down: bfloat16 [16, 2048, 512], P('fs', None, 'tp')
- mixed: bfloat16 [8192, 2048], P('fs', 'tp')
Inputs may be any that keep to these rules, and one draw needn't show every extreme that they name: `route_expert`: each row names two different experts of one group: for its group g both lie in g * 8 to g * 8 + 7, one of 2 groups. In each aligned block of 512 rows every expert is named by exactly 64 rows, half of them in each column.
All inputs are finite; a program needn't handle non-finite values.
Results may differ from a plain program's by a relative error of at most 0.014.
Values may be sent and summed in bfloat16 or wider, within the bound.
A program may use at most 64 MiB of HBM per device.

v0:
```python
import functools

import jax
import jax.numpy as jnp
from jax import lax
from jax.experimental import pallas as pl
from jax.experimental.pallas import tpu as pltpu
from jax.sharding import PartitionSpec as P

EPG = 8
TOP = 2
EPSILON = 1e-06
MESH = pl.DeviceIdType.MESH
F32, BF16 = jnp.float32, jnp.bfloat16
CHUNKS = 4
VMEM_LIMIT = 62 * 1024 * 1024


def index_grid(shape, dim):
    return lax.broadcasted_iota(jnp.int32, shape, dim).astype(F32)


def dot(a, b, contract=((1,), (0,)), **kw):
    return lax.dot_general(a, b, (contract, ((), ())), preferred_element_type=F32, **kw)


def send(src, dst, send_sem, recv_sem, **where):
    return pltpu.make_async_remote_copy(
        src_ref=src, dst_ref=dst, send_sem=send_sem, recv_sem=recv_sem, device_id=where, device_id_type=MESH
    )


def kernel(
    n, T, info, gain, tokens, w_gate, w_up, w_down, new_gate, new_up, new_down, mixed,
    wb, normed, info_t, s1s, i1s, s1r, i1r, s2s, x, sel, place, hid, ps, pr, eo, ret, ms, fin,
    w_snd, w_rcv, s1_snd, s1_rcv, i1_snd, i1_rcv, s2_snd, s2_rcv, tp_snd, tp_rcv,
    p_snd, p_rcv, r_snd, r_rcv, f_snd, f_rcv,
):
    me, tpi = lax.axis_index("fs"), lax.axis_index("tp")
    R, D = tokens.shape
    G = n // EPG
    g, i = me // EPG, me % EPG
    Rg, cap, Dt, K = R // G, TOP * R // n, D // T, D // n
    S = EPG * cap
    W = i1s.shape[2]
    C, Dc = ps.shape[1], ps.shape[4]

    barrier = pltpu.get_barrier_semaphore()

    def greet(k, c):
        pl.semaphore_signal(barrier, inc=1, device_id={"fs": (me + k) % n}, device_id_type=MESH)
        return c

    lax.fori_loop(1, n, greet, 0)
    for o in range(1, T):
        pl.semaphore_signal(barrier, inc=1, device_id={"tp": (tpi + o) % T}, device_id_type=MESH)
    pl.semaphore_wait(barrier, n - 1 + T - 1)

    def block(p):
        return pl.ds(pl.multiple_of(p * K, K), K)

    def slots(p):
        return pl.ds(pl.multiple_of(p * cap, cap), cap)

    def send_weights(m, src, dst, scaled):
        def cast(p, c):
            v = src[p]
            wb[m, p] = (v * gain[...] if scaled else v).astype(BF16)
            return c

        lax.fori_loop(0, n, cast, 0)

        def start(j, c):
            p = (me + j // 2 + (j % 2) * (n // 2)) % n
            send(wb.at[m, p], dst.at[block(me)], w_snd.at[m, p], w_rcv.at[m, me], fs=p).start()
            return c

        lax.fori_loop(1, n, start, 0)
        dst[block(me), :] = wb[m, me]

    def wait_weights(m, dst):
        def body(k, c):
            p = (me + k) % n
            send(wb.at[m, p], dst.at[block(p)], w_snd.at[m, p], w_rcv.at[m, p], fs=p).wait()
            return c

        lax.fori_loop(1, n, body, 0)

    step = 64

    def norm(b, c):
        rows = pl.ds(pl.multiple_of(b * step, step), step)
        v = tokens[rows, :].astype(F32)
        scale = lax.rsqrt(jnp.mean(v * v, axis=1, keepdims=True) + EPSILON)
        part = tokens[rows, pl.ds(pl.multiple_of(tpi * Dt, Dt), Dt)].astype(F32)
        normed[rows, :] = (part * scale).astype(BF16)
        return c

    lax.fori_loop(0, R // step, norm, 0)

    id0, id1 = info[0:1, :], info[1:2, :]
    gid = jnp.floor(id0 * (1.0 / EPG))
    experts = index_grid((n, R), 0)
    m0, m1 = experts == id0, experts == id1
    before = jnp.where(index_grid((R, R), 0) < index_grid((R, R), 1), 1.0, 0.0).astype(BF16)
    rank = dot(jnp.where(m0 | m1, 1.0, 0.0).astype(BF16), before)
    in_group = index_grid((max(G, 16), R), 0) == gid
    group_rank = dot(jnp.where(in_group, 1.0, 0.0).astype(BF16), before)
    slot0 = jnp.sum(jnp.where(m0, rank, 0.0), axis=0, keepdims=True) + (id0 - EPG * gid) * cap
    slot1 = jnp.sum(jnp.where(m1, rank, 0.0), axis=0, keepdims=True) + (id1 - EPG * gid) * cap
    pos = jnp.sum(jnp.where(in_group, group_rank, 0.0), axis=0, keepdims=True)
    line = index_grid((8, R), 0)
    table = info[...]
    for at, value in ((0, slot0), (1, slot1), (4, gid), (5, pos)):
        table = jnp.where(line == at, value, table)
    info_t[...] = table.T

    for k in range(G):
        q = (g + 1 + k) % G
        pick = jnp.where((index_grid((W, R), 0) == pos) & (gid == q.astype(F32)), 1.0, 0.0)
        info_q = dot(table, pick, ((1,), (1,)), precision=lax.Precision.HIGHEST)
        rows_q = dot(pick[:Rg].astype(BF16), normed[...]).astype(BF16)
        if k == G - 1:
            s1r[g] = rows_q
            i1r[g] = info_q
        else:
            s1s[q] = rows_q
            i1s[q] = info_q
            send(s1s.at[q], s1r.at[g], s1_snd.at[q], s1_rcv.at[g], fs=q * EPG + i).start()
            send(i1s.at[q], i1r.at[g], i1_snd.at[q], i1_rcv.at[g], fs=q * EPG + i).start()

    send_weights(0, w_gate, new_gate, True)

    for k in (G - 1, *range(G - 1)):
        h = (g + 1 + k) % G
        if k < G - 1:
            send(s1s.at[h], s1r.at[h], s1_snd.at[h], s1_rcv.at[h], fs=h * EPG + i).wait()
            send(i1s.at[h], i1r.at[h], i1_snd.at[h], i1_rcv.at[h], fs=h * EPG + i).wait()
        slot_q = i1r[h]
        grid = index_grid((S, Rg), 0)
        spread = (grid == slot_q[0:1, :Rg]) | (grid == slot_q[1:2, :Rg])
        s2s[h] = dot(jnp.where(spread, 1.0, 0.0).astype(BF16), s1r[h]).astype(BF16)
        for j in range(1, EPG):
            p = (i + j) % EPG
            send(
                s2s.at[h, slots(p)], x.at[tpi, h, slots(i)], s2_snd.at[h, p], s2_rcv.at[h, i], fs=g * EPG + p
            ).start()
        x[tpi, h, slots(i), :] = s2s[h, slots(i), :]

    send_weights(1, w_up, new_up, True)
    send_weights(2, w_down, new_down, False)

    for k in (G - 1, *range(G - 1)):
        h = (g + 1 + k) % G
        for j in range(1, EPG):
            p = (i + j) % EPG
            send(
                s2s.at[h, slots(p)], x.at[tpi, h, slots(p)], s2_snd.at[h, p], s2_rcv.at[h, p], fs=g * EPG + p
            ).wait()
        for o in range(1, T):
            send(x.at[tpi, h], x.at[tpi, h], tp_snd.at[h, o], tp_rcv.at[h, o], tp=(tpi + o) % T).start()
    for k in range(G):
        h = (g + 1 + k) % G
        for o in range(1, T):
            t = (tpi + T - o) % T
            send(x.at[t, h], x.at[t, h], tp_snd.at[h, o], tp_rcv.at[h, o], tp=(tpi + o) % T).wait()

    for k in range(G):
        h = (g + 1 + k) % G
        cols = i1r[h].T[:Rg]
        grid = index_grid((Rg, S), 1)
        for c in range(TOP):
            sel[h, c] = jnp.where(grid == cols[:, c : c + 1], 1.0, 0.0).astype(BF16)
        grid = index_grid((R, Rg), 1)
        here = (grid == info_t[:, 5:6]) & (info_t[:, 4:5] == h.astype(F32))
        place[h] = jnp.where(here, 1.0, 0.0).astype(BF16)

    wait_weights(0, new_gate)
    wait_weights(1, new_up)

    tile = min(S, 256)
    for k in range(G):
        h = (g + 1 + k) % G

        def expert(b, c):
            rows = pl.ds(pl.multiple_of(b * tile, tile), tile)
            gate_pre = up_pre = 0.0
            for t in range(T):
                part = x[t, h, rows, :]
                gate_pre += dot(part, new_gate[t * Dt : (t + 1) * Dt, :])
                up_pre += dot(part, new_up[t * Dt : (t + 1) * Dt, :])
            hid[h, rows, :] = (gate_pre / (1.0 + jnp.exp(-gate_pre)) * up_pre).astype(BF16)
            return c

        lax.fori_loop(0, S // tile, expert, 0)

    wait_weights(2, new_down)

    def sum_units(c, h):
        for t in range(T):
            at = t * Dt + c * Dc
            ps[t, c, h] = dot(hid[h], new_down[at : at + Dc, :], ((1,), (1,))).astype(BF16)
        for o in range(1, T):
            t = (tpi + o) % T
            send(ps.at[t, c, h], pr.at[o, c, h], p_snd.at[c, h, o], p_rcv.at[c, h, o], tp=t).start()

    def hand_back(c, h):
        total = ps[tpi, c, h].astype(F32)
        for o in range(1, T):
            t = (tpi + o) % T
            send(ps.at[t, c, h], pr.at[o, c, h], p_snd.at[c, h, o], p_rcv.at[c, h, o], tp=t).wait()
            total += pr[o, c, h].astype(F32)
        eo[c, h] = total.astype(BF16)
        for j in range(1, EPG):
            p = (i + j) % EPG
            send(
                eo.at[c, h, slots(p)], ret.at[c, h, slots(i)], r_snd.at[c, h, p], r_rcv.at[c, h, i], fs=g * EPG + p
            ).start()
        ret[c, h, slots(i), :] = eo[c, h, slots(i), :]

    def mix(c, h, last):
        for j in range(1, EPG):
            p = (i + j) % EPG
            send(
                eo.at[c, h, slots(p)], ret.at[c, h, slots(p)], r_snd.at[c, h, p], r_rcv.at[c, h, p], fs=g * EPG + p
            ).wait()
        cols = i1r[h].T[:Rg]
        outs = ret[c, h]
        both = (cols[:, 2:3] * dot(sel[h, 0], outs) + cols[:, 3:4] * dot(sel[h, 1], outs)).astype(BF16)
        if last:
            fin[c, g] = both
        else:
            ms[c, h] = both
            send(ms.at[c, h], fin.at[c, g], f_snd.at[c, h], f_rcv.at[c, g], fs=h * EPG + i).start()

    steps = [(c, (g + 1 + k) % G, k == G - 1) for k in range(G) for c in range(C)]
    for s in range(len(steps) + 3):
        if s < len(steps):
            sum_units(*steps[s][:2])
        if 1 <= s <= len(steps):
            hand_back(*steps[s - 1][:2])
        if s >= 3:
            mix(*steps[s - 3])

    for c in range(C):
        total = 0.0
        for k in (G - 1, *range(G - 1)):
            q = (g + 1 + k) % G
            if k < G - 1:
                send(ms.at[c, q], fin.at[c, q], f_snd.at[c, q], f_rcv.at[c, q], fs=q * EPG + i).wait()
            total += dot(place[q], fin[c, q])
        mixed[:, c * Dc : (c + 1) * Dc] = total.astype(BF16)


def local(tokens, norm_gain, w_gate, w_up, w_down, route_expert, group_prob, pair_logit):
    n, T = lax.axis_size("fs"), lax.axis_size("tp")
    R, D = tokens.shape
    F = w_gate.shape[2]
    G = n // EPG
    Rg, cap, Dt = R // G, TOP * R // n, D // T
    S, W = EPG * cap, max(Rg, 128)
    Dc = min(Dt, max(Dt // CHUNKS, 128))
    C = Dt // Dc
    gap = pair_logit[:, 0] - pair_logit[:, 1]
    none = jnp.zeros_like(gap)
    ids = route_expert.astype(F32)
    info = jnp.stack(
        [ids[:, 0], ids[:, 1], group_prob * jax.nn.sigmoid(gap), group_prob * jax.nn.sigmoid(-gap)] + [none] * 4
    )
    vmem = pl.BlockSpec(memory_space=pltpu.VMEM)
    sem = pltpu.SemaphoreType.DMA
    weights = jax.ShapeDtypeStruct((D, F), BF16)
    gate, up, down, mixed = pl.pallas_call(
        functools.partial(kernel, n, T),
        out_shape=[weights, weights, weights, jax.ShapeDtypeStruct((R, Dt), BF16)],
        in_specs=[vmem] * 6,
        out_specs=[vmem] * 4,
        scratch_shapes=[
            pltpu.VMEM((3, n, D // n, F), BF16),
            pltpu.VMEM((R, Dt), BF16),
            pltpu.VMEM((R, 8), F32),
            pltpu.VMEM((G, Rg, Dt), BF16),
            pltpu.VMEM((G, 8, W), F32),
            pltpu.VMEM((G, Rg, Dt), BF16),
            pltpu.VMEM((G, 8, W), F32),
            pltpu.VMEM((G, S, Dt), BF16),
            pltpu.VMEM((T, G, S, Dt), BF16),
            pltpu.VMEM((G, TOP, Rg, S), BF16),
            pltpu.VMEM((G, R, Rg), BF16),
            pltpu.VMEM((G, S, F), BF16),
            pltpu.VMEM((T, C, G, S, Dc), BF16),
            pltpu.VMEM((T, C, G, S, Dc), BF16),
            pltpu.VMEM((C, G, S, Dc), BF16),
            pltpu.VMEM((C, G, S, Dc), BF16),
            pltpu.VMEM((C, G, Rg, Dc), BF16),
            pltpu.VMEM((C, G, Rg, Dc), BF16),
            sem((3, n)), sem((3, n)),
            sem((G,)), sem((G,)), sem((G,)), sem((G,)),
            sem((G, EPG)), sem((G, EPG)),
            sem((G, T)), sem((G, T)), sem((C, G, T)), sem((C, G, T)),
            sem((C, G, EPG)), sem((C, G, EPG)),
            sem((C, G)), sem((C, G)),
        ],
        compiler_params=pltpu.CompilerParams(
            collective_id=0, has_side_effects=True, vmem_limit_bytes=VMEM_LIMIT
        ),
    )(info, norm_gain[:, None], tokens, w_gate, w_up, w_down)
    return gate[None], up[None], down[None], mixed


def solution(mesh):
    placed = (
        P("fs", None),
        P("fs"),
        P(None, "fs", "tp"),
        P(None, "fs", "tp"),
        P(None, "fs", "tp"),
        P("fs", None),
        P("fs"),
        P("fs", None),
    )
    return jax.shard_map(
        local,
        mesh=mesh,
        in_specs=placed,
        out_specs=(P("fs", None, "tp"), P("fs", None, "tp"), P("fs", None, "tp"), P("fs", "tp")),
        check_vma=False,
    )
```

profile of v0, /device:TPU:0, one launch (start us, length us, event | category | flops | bytes accessed | tf_op | source)
XLA Modules:
  0.0 159.5 jit_solution(14155176870494074618)
XLA Ops:
  0.6 0.7 convert_element_type.3
  1.3 0.8 add_divide_fusion
  2.1 0.7 fusion
  2.8 0.6 stack.15.info
  3.4 1.4 copy.12.gain
  4.8 149.3 %shard_map.111 = (bf16[2048,256]{1,0:T(8,128)(2,1)}, bf16[2048,256]{1,0:T(8,128)(2,1)}, bf16[2048,256]{1,0:T(8,128)(2,1)}, bf16[512,1024]{1,0:T(8,128)(2,1)}) custom-call(f32[8,512]{1,0:T(8,128)} %stack.15.info, f32[128,1]{1,0:T(8,128)} %copy.12.gain, bf16[512,2048]{1,0:T(8,128)(2,1)} %tokens.1, f32[16,128,256]{2,1,0:T(8,128)} %w_gate.1, ...), custom_call_target="tpu_custom_call" | custom-call | tf_op jit(solution)/shard_map/pallas_call | solution.py:273
  154.2 0.0 copy-start.2
  154.2 0.0 copy-start.1
  154.2 2.4 %copy.17 = bf16[1,2048,256]{2,1,0:T(8,128)(2,1)} copy(bf16[1,2048,256]{2,1,0:T(8,128)(2,1)} %bitcast.14) | data formatting | bytes 2097152
  156.6 0.0 copy-done.2
  156.6 0.0 copy-start
  156.6 1.0 copy.18
  157.6 0.0 copy-done.1
  157.6 1.0 copy.19
  158.5 0.0 copy-done
  158.5 1.0 copy.20
  (3 shorter events, 0.0 us)
Async XLA Ops:
  154.2 2.4 %copy-start.2 = (bf16[2048,256]{1,0:T(8,128)(2,1)S(1)}, bf16[2048,256]{1,0:T(8,128)(2,1)}, u32[]{:S(2)}) copy-start(bf16[2048,256]{1,0:T(8,128)(2,1)} %get-tuple-element.9) | copy-start | bytes 3145732
  154.2 3.4 %copy-start.1 = (bf16[2048,256]{1,0:T(8,128)(2,1)S(1)}, bf16[2048,256]{1,0:T(8,128)(2,1)}, u32[]{:S(2)}) copy-start(bf16[2048,256]{1,0:T(8,128)(2,1)} %get-tuple-element.10) | copy-start | bytes 3145732
  156.6 1.9 %copy-start = (bf16[512,1024]{1,0:T(8,128)(2,1)S(1)}, bf16[512,1024]{1,0:T(8,128)(2,1)}, u32[]{:S(2)}) copy-start(bf16[512,1024]{1,0:T(8,128)(2,1)} %get-tuple-element.25) | copy-start | bytes 3145732
where the time goes:
time: 160 us
  Pallas kernels  149 us (93%)
  local copies, waits for them, and re-layouts  7.36 us (5%)
  other arithmetic  2.16 us (1%)
    pallas_call x1, Pallas kernels, local(): pl.pallas_call(functools.partial(kernel, n, T), out_shape=[weights, weigh...  149 us
    unnamed x10, local copies, waits for them, and re-layouts  5.33 us

commit v1 on v0

--- a/solution.py
+++ b/solution.py
@@ -30,10 +30,22 @@
     )
 
 
+def partner(me, j, n):
+    if n & (n - 1):
+        return (me + j) % n
+    p, bit = 0, 1
+    while bit < n:
+        here = (me // bit) % 2
+        p = p + bit * (1 - here if j & bit else here)
+        bit *= 2
+    return p
+
+
 def kernel(
-    n, T, info, gain, tokens, w_gate, w_up, w_down, new_gate, new_up, new_down, mixed,
+    n, T, ids, gain, prob, logit, tokens_in, gate_in, up_in, down_in, gate_out, up_out, down_out, mixed_out,
+    tokens, w_gate, w_up, w_down, new_gate, new_up, new_down, mixed,
     wb, normed, info_t, s1s, i1s, s1r, i1r, s2s, x, sel, place, hid, ps, pr, eo, ret, ms, fin,
-    w_snd, w_rcv, s1_snd, s1_rcv, i1_snd, i1_rcv, s2_snd, s2_rcv, tp_snd, tp_rcv,
+    in_sem, out_sem, w_snd, w_rcv, s1_snd, s1_rcv, i1_snd, i1_rcv, s2_snd, s2_rcv, tp_snd, tp_rcv,
     p_snd, p_rcv, r_snd, r_rcv, f_snd, f_rcv,
 ):
     me, tpi = lax.axis_index("fs"), lax.axis_index("tp")
@@ -54,7 +66,15 @@
     lax.fori_loop(1, n, greet, 0)
     for o in range(1, T):
         pl.semaphore_signal(barrier, inc=1, device_id={"tp": (tpi + o) % T}, device_id_type=MESH)
-    pl.semaphore_wait(barrier, n - 1 + T - 1)
+
+    loads = [
+        pltpu.make_async_copy(src, dst, in_sem.at[k])
+        for k, (src, dst) in enumerate(
+            ((tokens_in, tokens), (gate_in, w_gate), (up_in, w_up), (down_in, w_down))
+        )
+    ]
+    for load in loads:
+        load.start()
 
     def block(p):
         return pl.ds(pl.multiple_of(p * K, K), K)
@@ -62,20 +82,24 @@
     def slots(p):
         return pl.ds(pl.multiple_of(p * cap, cap), cap)
 
-    def send_weights(m, src, dst, scaled):
+    diagonal = index_grid((K, K), 0) == index_grid((K, K), 1)
+    gains = jnp.sum(jnp.where(diagonal, gain[...], 0.0), axis=1, keepdims=True)
+
+    def cast_weights(m, src, scaled):
         def cast(p, c):
             v = src[p]
-            wb[m, p] = (v * gain[...] if scaled else v).astype(BF16)
+            wb[m, p] = (v * gains if scaled else v).astype(BF16)
             return c
 
+        loads[1 + m].wait()
         lax.fori_loop(0, n, cast, 0)
 
-        def start(j, c):
-            p = (me + j // 2 + (j % 2) * (n // 2)) % n
+    order = [*range(n // 2, n), *range(1, n // 2)]
+
+    def send_weights(m, dst):
+        for j in order:
+            p = partner(me, j, n)
             send(wb.at[m, p], dst.at[block(me)], w_snd.at[m, p], w_rcv.at[m, me], fs=p).start()
-            return c
-
-        lax.fori_loop(1, n, start, 0)
         dst[block(me), :] = wb[m, me]
 
     def wait_weights(m, dst):
@@ -86,19 +110,8 @@
 
         lax.fori_loop(1, n, body, 0)
 
-    step = 64
-
-    def norm(b, c):
-        rows = pl.ds(pl.multiple_of(b * step, step), step)
-        v = tokens[rows, :].astype(F32)
-        scale = lax.rsqrt(jnp.mean(v * v, axis=1, keepdims=True) + EPSILON)
-        part = tokens[rows, pl.ds(pl.multiple_of(tpi * Dt, Dt), Dt)].astype(F32)
-        normed[rows, :] = (part * scale).astype(BF16)
-        return c
-
-    lax.fori_loop(0, R // step, norm, 0)
-
-    id0, id1 = info[0:1, :], info[1:2, :]
+    id0, id1 = ids[0:1, :].astype(F32), ids[1:2, :].astype(F32)
+    gap = logit[0:1, :] - logit[1:2, :]
     gid = jnp.floor(id0 * (1.0 / EPG))
     experts = index_grid((n, R), 0)
     m0, m1 = experts == id0, experts == id1
@@ -110,10 +123,24 @@
     slot1 = jnp.sum(jnp.where(m1, rank, 0.0), axis=0, keepdims=True) + (id1 - EPG * gid) * cap
     pos = jnp.sum(jnp.where(in_group, group_rank, 0.0), axis=0, keepdims=True)
     line = index_grid((8, R), 0)
-    table = info[...]
-    for at, value in ((0, slot0), (1, slot1), (4, gid), (5, pos)):
+    table = jnp.zeros((8, R), F32)
+    rows = (slot0, slot1, prob[...] * jax.nn.sigmoid(gap), prob[...] * jax.nn.sigmoid(-gap), gid, pos)
+    for at, value in enumerate(rows):
         table = jnp.where(line == at, value, table)
     info_t[...] = table.T
+
+    step = 64
+
+    def norm(b, c):
+        rows = pl.ds(pl.multiple_of(b * step, step), step)
+        v = tokens[rows, :].astype(F32)
+        scale = lax.rsqrt(jnp.mean(v * v, axis=1, keepdims=True) + EPSILON)
+        part = tokens[rows, pl.ds(pl.multiple_of(tpi * Dt, Dt), Dt)].astype(F32)
+        normed[rows, :] = (part * scale).astype(BF16)
+        return c
+
+    loads[0].wait()
+    lax.fori_loop(0, R // step, norm, 0)
 
     for k in range(G):
         q = (g + 1 + k) % G
@@ -126,29 +153,49 @@
         else:
             s1s[q] = rows_q
             i1s[q] = info_q
-            send(s1s.at[q], s1r.at[g], s1_snd.at[q], s1_rcv.at[g], fs=q * EPG + i).start()
-            send(i1s.at[q], i1r.at[g], i1_snd.at[q], i1_rcv.at[g], fs=q * EPG + i).start()
-
-    send_weights(0, w_gate, new_gate, True)
-
-    for k in (G - 1, *range(G - 1)):
-        h = (g + 1 + k) % G
-        if k < G - 1:
-            send(s1s.at[h], s1r.at[h], s1_snd.at[h], s1_rcv.at[h], fs=h * EPG + i).wait()
-            send(i1s.at[h], i1r.at[h], i1_snd.at[h], i1_rcv.at[h], fs=h * EPG + i).wait()
+
+    cast_weights(0, w_gate, True)
+    pl.semaphore_wait(barrier, n - 1 + T - 1)
+
+    for k in range(G - 1):
+        q = (g + 1 + k) % G
+        send(i1s.at[q], i1r.at[g], i1_snd.at[q], i1_rcv.at[g], fs=q * EPG + i).start()
+        send(s1s.at[q], s1r.at[g], s1_snd.at[q], s1_rcv.at[g], fs=q * EPG + i).start()
+    send_weights(0, new_gate)
+
+    def dispatch(h):
         slot_q = i1r[h]
         grid = index_grid((S, Rg), 0)
         spread = (grid == slot_q[0:1, :Rg]) | (grid == slot_q[1:2, :Rg])
         s2s[h] = dot(jnp.where(spread, 1.0, 0.0).astype(BF16), s1r[h]).astype(BF16)
         for j in range(1, EPG):
-            p = (i + j) % EPG
+            p = partner(i, j, EPG)
             send(
                 s2s.at[h, slots(p)], x.at[tpi, h, slots(i)], s2_snd.at[h, p], s2_rcv.at[h, i], fs=g * EPG + p
             ).start()
         x[tpi, h, slots(i), :] = s2s[h, slots(i), :]
 
-    send_weights(1, w_up, new_up, True)
-    send_weights(2, w_down, new_down, False)
+    dispatch(g)
+    cast_weights(1, w_up, True)
+    send_weights(1, new_up)
+    cast_weights(2, w_down, False)
+
+    for k in range(G - 1):
+        h = (g + 1 + k) % G
+        send(i1s.at[h], i1r.at[h], i1_snd.at[h], i1_rcv.at[h], fs=h * EPG + i).wait()
+        send(s1s.at[h], s1r.at[h], s1_snd.at[h], s1_rcv.at[h], fs=h * EPG + i).wait()
+        dispatch(h)
+    send_weights(2, new_down)
+
+    for k in range(G):
+        h = (g + 1 + k) % G
+        cols = i1r[h].T[:Rg]
+        grid = index_grid((Rg, S), 1)
+        for c in range(TOP):
+            sel[h, c] = jnp.where(grid == cols[:, c : c + 1], 1.0, 0.0).astype(BF16)
+        grid = index_grid((R, Rg), 1)
+        here = (grid == info_t[:, 5:6]) & (info_t[:, 4:5] == h.astype(F32))
+        place[h] = jnp.where(here, 1.0, 0.0).astype(BF16)
 
     for k in (G - 1, *range(G - 1)):
         h = (g + 1 + k) % G
@@ -165,18 +212,14 @@
             t = (tpi + T - o) % T
             send(x.at[t, h], x.at[t, h], tp_snd.at[h, o], tp_rcv.at[h, o], tp=(tpi + o) % T).wait()
 
-    for k in range(G):
-        h = (g + 1 + k) % G
-        cols = i1r[h].T[:Rg]
-        grid = index_grid((Rg, S), 1)
-        for c in range(TOP):
-            sel[h, c] = jnp.where(grid == cols[:, c : c + 1], 1.0, 0.0).astype(BF16)
-        grid = index_grid((R, Rg), 1)
-        here = (grid == info_t[:, 5:6]) & (info_t[:, 4:5] == h.astype(F32))
-        place[h] = jnp.where(here, 1.0, 0.0).astype(BF16)
-
+    stores = [
+        pltpu.make_async_copy(src, dst, out_sem.at[k])
+        for k, (src, dst) in enumerate(((new_gate, gate_out), (new_up, up_out), (new_down, down_out)))
+    ]
     wait_weights(0, new_gate)
+    stores[0].start()
     wait_weights(1, new_up)
+    stores[1].start()
 
     tile = min(S, 256)
     for k in range(G):
@@ -195,6 +238,7 @@
         lax.fori_loop(0, S // tile, expert, 0)
 
     wait_weights(2, new_down)
+    stores[2].start()
 
     def sum_units(c, h):
         for t in range(T):
@@ -212,7 +256,7 @@
             total += pr[o, c, h].astype(F32)
         eo[c, h] = total.astype(BF16)
         for j in range(1, EPG):
-            p = (i + j) % EPG
+            p = partner(i, j, EPG)
             send(
                 eo.at[c, h, slots(p)], ret.at[c, h, slots(i)], r_snd.at[c, h, p], r_rcv.at[c, h, i], fs=g * EPG + p
             ).start()
@@ -250,6 +294,33 @@
                 send(ms.at[c, q], fin.at[c, q], f_snd.at[c, q], f_rcv.at[c, q], fs=q * EPG + i).wait()
             total += dot(place[q], fin[c, q])
         mixed[:, c * Dc : (c + 1) * Dc] = total.astype(BF16)
+        stores.append(
+            pltpu.make_async_copy(
+                mixed.at[:, c * Dc : (c + 1) * Dc], mixed_out.at[:, c * Dc : (c + 1) * Dc], out_sem.at[3 + c]
+            )
+        )
+        stores[-1].start()
+    for store in stores:
+        store.wait()
+
+
+def hand_over(count, *refs):
+    sources, results, rooms = refs[:4], refs[4:8], refs[8:12]
+    arrived, left = refs[12:]
+    into, out = [], []
+    for a, (source, room, result) in enumerate(zip(sources, rooms, results)):
+        height = source.shape[0] // count
+        for b in range(count):
+            rows = pl.ds(b * height, height)
+            into.append(pltpu.make_async_copy(source.at[rows], room.at[rows], arrived.at[a, b]))
+            out.append(pltpu.make_async_copy(room.at[rows], result.at[rows], left.at[a, b]))
+    for copy in into:
+        copy.start()
+    for first, second in zip(into, out):
+        first.wait()
+        second.start()
+    for copy in out:
+        copy.wait()
 
 
 def local(tokens, norm_gain, w_gate, w_up, w_down, route_expert, group_prob, pair_logit):
@@ -261,21 +332,25 @@
     S, W = EPG * cap, max(Rg, 128)
     Dc = min(Dt, max(Dt // CHUNKS, 128))
     C = Dt // Dc
-    gap = pair_logit[:, 0] - pair_logit[:, 1]
-    none = jnp.zeros_like(gap)
-    ids = route_expert.astype(F32)
-    info = jnp.stack(
-        [ids[:, 0], ids[:, 1], group_prob * jax.nn.sigmoid(gap), group_prob * jax.nn.sigmoid(-gap)] + [none] * 4
-    )
     vmem = pl.BlockSpec(memory_space=pltpu.VMEM)
+    hbm = pl.BlockSpec(memory_space=pl.ANY)
     sem = pltpu.SemaphoreType.DMA
     weights = jax.ShapeDtypeStruct((D, F), BF16)
-    gate, up, down, mixed = pl.pallas_call(
+    shapes = [weights, weights, weights, jax.ShapeDtypeStruct((R, Dt), BF16)]
+    results = pl.pallas_call(
         functools.partial(kernel, n, T),
-        out_shape=[weights, weights, weights, jax.ShapeDtypeStruct((R, Dt), BF16)],
-        in_specs=[vmem] * 6,
-        out_specs=[vmem] * 4,
+        out_shape=shapes,
+        in_specs=[vmem] * 4 + [hbm] * 4,
+        out_specs=[hbm] * 4,
         scratch_shapes=[
+            pltpu.VMEM((R, D), BF16),
+            pltpu.VMEM(w_gate.shape, F32),
+            pltpu.VMEM(w_up.shape, F32),
+            pltpu.VMEM(w_down.shape, F32),
+            pltpu.VMEM((D, F), BF16),
+            pltpu.VMEM((D, F), BF16),
+            pltpu.VMEM((D, F), BF16),
+            pltpu.VMEM((R, Dt), BF16),
             pltpu.VMEM((3, n, D // n, F), BF16),
             pltpu.VMEM((R, Dt), BF16),
             pltpu.VMEM((R, 8), F32),
@@ -294,6 +369,7 @@
             pltpu.VMEM((C, G, S, Dc), BF16),
             pltpu.VMEM((C, G, Rg, Dc), BF16),
             pltpu.VMEM((C, G, Rg, Dc), BF16),
+            sem((4,)), sem((3 + C,)),
             sem((3, n)), sem((3, n)),
             sem((G,)), sem((G,)), sem((G,)), sem((G,)),
             sem((G, EPG)), sem((G, EPG)),
@@ -304,7 +380,18 @@
         compiler_params=pltpu.CompilerParams(
             collective_id=0, has_side_effects=True, vmem_limit_bytes=VMEM_LIMIT
         ),
-    )(info, norm_gain[:, None], tokens, w_gate, w_up, w_down)
+    )(
+        route_expert.T, norm_gain[None, :], group_prob[None, :], pair_logit.T,
+        tokens, w_gate, w_up, w_down,
+    )
+    parts = 2
+    gate, up, down, mixed = pl.pallas_call(
+        functools.partial(hand_over, parts),
+        out_shape=shapes,
+        in_specs=[hbm] * 4,
+        out_specs=[hbm] * 4,
+        scratch_shapes=[pltpu.VMEM(s.shape, s.dtype) for s in shapes] + [sem((4, parts)), sem((4, parts))],
+    )(*results)
     return gate[None], up[None], down[None], mixed
 
 

time: 160 us -> 150 us (0.938)
  local copies, waits for them, and re-layouts: 7.36 us -> 0 us
  other arithmetic: 2.16 us -> 0 us
    unnamed x10 -> x0, local copies, waits for them, and re-layouts: 5.33 us -> none
    pallas_call x1 -> x2, Pallas kernels: 149 us -> 149 us  [the longest x1 145 us: local(): pl.pallas_call(functools.partial(kernel, n, T), out_shape=shapes, in_spec...]
where the time goes in v1:
time: 150 us; the launch traced here: 149 us
  Pallas kernels  149 us (99%)
    pallas_call x1, Pallas kernels, local(): pl.pallas_call(functools.partial(kernel, n, T), out_shape=shapes, in_spec...  145 us
    pallas_call x1, Pallas kernels, local(): pl.pallas_call(functools.partial(hand_over, parts), out_shape=shapes, in_...  3.58 us

profile of v1, /device:TPU:0, one launch (start us, length us, event | category | flops | bytes accessed | tf_op | source)
XLA Modules:
  0.0 149.4 jit_solution(9402226766914792079)
XLA Ops:
  0.6 145.2 %shard_map.111 = (bf16[2048,256]{1,0:T(8,128)(2,1)}, bf16[2048,256]{1,0:T(8,128)(2,1)}, bf16[2048,256]{1,0:T(8,128)(2,1)}, bf16[512,1024]{1,0:T(8,128)(2,1)}) custom-call(s32[2,512]{1,0:T(2,128)} %bitcast.7, f32[1,128]{1,0:T(1,128)} %bitcast.10, f32[1,512]{1,0:T(1,128)} %bitcast.9, f32[2,512]{1,0:T(2,128)} %bitcast.8, bf16[512,2048]{1,0:T(8,128)(2,1)} %tokens_in.1, ...), custom_call_target="tpu_custom_call" | custom-call | tf_op jit(solution)/shard_map/pallas_call | solution.py:340
  145.8 3.6 %shard_map.112 = (bf16[2048,256]{1,0:T(8,128)(2,1)}, bf16[2048,256]{1,0:T(8,128)(2,1)}, bf16[2048,256]{1,0:T(8,128)(2,1)}, bf16[512,1024]{1,0:T(8,128)(2,1)}) custom-call(bf16[2048,256]{1,0:T(8,128)(2,1)} %get-tuple-element.12.refs_0_, bf16[2048,256]{1,0:T(8,128)(2,1)} %get-tuple-element.13.refs_1_, bf16[2048,256]{1,0:T(8,128)(2,1)} %get-tuple-element.14.refs_2_, ...), custom_call_target="tpu_custom_call" | custom-call | tf_op jit(solution)/shard_map/pallas_call | solution.py:388

commit v2 on v1

--- a/solution.py
+++ b/solution.py
@@ -94,21 +94,27 @@
         loads[1 + m].wait()
         lax.fori_loop(0, n, cast, 0)
 
-    order = [*range(n // 2, n), *range(1, n // 2)]
-
-    def send_weights(m, dst):
+    def send_weights(m, dst, order):
         for j in order:
             p = partner(me, j, n)
             send(wb.at[m, p], dst.at[block(me)], w_snd.at[m, p], w_rcv.at[m, me], fs=p).start()
-        dst[block(me), :] = wb[m, me]
-
-    def wait_weights(m, dst):
+
+    near, far = range(1, EPG), range(EPG, n)
+
+    def weights_from(m, dst, p):
+        return send(wb.at[m, p], dst.at[block(p)], w_snd.at[m, p], w_rcv.at[m, p], fs=p)
+
+    def wait_weights(m, dst, first, count):
         def body(k, c):
-            p = (me + k) % n
-            send(wb.at[m, p], dst.at[block(p)], w_snd.at[m, p], w_rcv.at[m, p], fs=p).wait()
+            p = first + k
+
+            @pl.when(p != me)
+            def _():
+                weights_from(m, dst, p).wait_recv()
+
             return c
 
-        lax.fori_loop(1, n, body, 0)
+        lax.fori_loop(0, count, body, 0)
 
     id0, id1 = ids[0:1, :].astype(F32), ids[1:2, :].astype(F32)
     gap = logit[0:1, :] - logit[1:2, :]
@@ -161,7 +167,6 @@
         q = (g + 1 + k) % G
         send(i1s.at[q], i1r.at[g], i1_snd.at[q], i1_rcv.at[g], fs=q * EPG + i).start()
         send(s1s.at[q], s1r.at[g], s1_snd.at[q], s1_rcv.at[g], fs=q * EPG + i).start()
-    send_weights(0, new_gate)
 
     def dispatch(h):
         slot_q = i1r[h]
@@ -176,16 +181,22 @@
         x[tpi, h, slots(i), :] = s2s[h, slots(i), :]
 
     dispatch(g)
+    send_weights(0, new_gate, far)
     cast_weights(1, w_up, True)
-    send_weights(1, new_up)
+    send_weights(1, new_up, far)
+    send_weights(0, new_gate, near)
+    send_weights(1, new_up, near)
     cast_weights(2, w_down, False)
+    for m, dst in enumerate((new_gate, new_up, new_down)):
+        dst[block(me), :] = wb[m, me]
 
     for k in range(G - 1):
         h = (g + 1 + k) % G
         send(i1s.at[h], i1r.at[h], i1_snd.at[h], i1_rcv.at[h], fs=h * EPG + i).wait()
         send(s1s.at[h], s1r.at[h], s1_snd.at[h], s1_rcv.at[h], fs=h * EPG + i).wait()
         dispatch(h)
-    send_weights(2, new_down)
+    send_weights(2, new_down, near)
+    send_weights(2, new_down, far)
 
     for k in range(G):
         h = (g + 1 + k) % G
@@ -197,34 +208,23 @@
         here = (grid == info_t[:, 5:6]) & (info_t[:, 4:5] == h.astype(F32))
         place[h] = jnp.where(here, 1.0, 0.0).astype(BF16)
 
-    for k in (G - 1, *range(G - 1)):
-        h = (g + 1 + k) % G
+    def exchange(h):
         for j in range(1, EPG):
-            p = (i + j) % EPG
+            p = partner(i, j, EPG)
             send(
                 s2s.at[h, slots(p)], x.at[tpi, h, slots(p)], s2_snd.at[h, p], s2_rcv.at[h, p], fs=g * EPG + p
-            ).wait()
+            ).wait_recv()
         for o in range(1, T):
             send(x.at[tpi, h], x.at[tpi, h], tp_snd.at[h, o], tp_rcv.at[h, o], tp=(tpi + o) % T).start()
-    for k in range(G):
-        h = (g + 1 + k) % G
+
+    def exchanged(h):
         for o in range(1, T):
             t = (tpi + T - o) % T
-            send(x.at[t, h], x.at[t, h], tp_snd.at[h, o], tp_rcv.at[h, o], tp=(tpi + o) % T).wait()
-
-    stores = [
-        pltpu.make_async_copy(src, dst, out_sem.at[k])
-        for k, (src, dst) in enumerate(((new_gate, gate_out), (new_up, up_out), (new_down, down_out)))
-    ]
-    wait_weights(0, new_gate)
-    stores[0].start()
-    wait_weights(1, new_up)
-    stores[1].start()
+            send(x.at[t, h], x.at[t, h], tp_snd.at[h, o], tp_rcv.at[h, o], tp=(tpi + o) % T).wait_recv()
 
     tile = min(S, 256)
-    for k in range(G):
-        h = (g + 1 + k) % G
-
+
+    def apply_experts(h):
         def expert(b, c):
             rows = pl.ds(pl.multiple_of(b * tile, tile), tile)
             gate_pre = up_pre = 0.0
@@ -237,37 +237,57 @@
 
         lax.fori_loop(0, S // tile, expert, 0)
 
-    wait_weights(2, new_down)
-    stores[2].start()
-
-    def sum_units(c, h):
-        for t in range(T):
-            at = t * Dt + c * Dc
-            ps[t, c, h] = dot(hid[h], new_down[at : at + Dc, :], ((1,), (1,))).astype(BF16)
+    stores = [
+        pltpu.make_async_copy(src, dst, out_sem.at[k])
+        for k, (src, dst) in enumerate(((new_gate, gate_out), (new_up, up_out), (new_down, down_out)))
+    ]
+    others = [(g + 1 + k) % G for k in range(G - 1)]
+    exchange(g)
+    for h in others:
+        exchange(h)
+    wait_weights(0, new_gate, 0, n)
+    stores[0].start()
+    wait_weights(1, new_up, 0, n)
+    stores[1].start()
+    exchanged(g)
+    apply_experts(g)
+    for h in others:
+        exchanged(h)
+        apply_experts(h)
+
+    def partial(h, c, o, t):
+        return send(ps.at[o, c, h], pr.at[o, c, h], p_snd.at[c, h, o], p_rcv.at[c, h, o], tp=t)
+
+    def sum_units(t, o, c, h):
+        rows = pl.ds(pl.multiple_of(t * Dt + c * Dc, Dc), Dc)
+        ps[o, c, h] = dot(hid[h], new_down[rows, :], ((1,), (1,))).astype(BF16)
+
+        @pl.when(t != tpi)
+        def _():
+            partial(h, c, o, t).start()
+
+    def return_to(h, c, p, q):
+        return send(
+            eo.at[c, h, slots(p)], ret.at[c, h, slots(q)], r_snd.at[c, h, p], r_rcv.at[c, h, q], fs=g * EPG + p
+        )
+
+    def hand_back(c, h):
+        total = ps[0, c, h].astype(F32)
         for o in range(1, T):
-            t = (tpi + o) % T
-            send(ps.at[t, c, h], pr.at[o, c, h], p_snd.at[c, h, o], p_rcv.at[c, h, o], tp=t).start()
-
-    def hand_back(c, h):
-        total = ps[tpi, c, h].astype(F32)
-        for o in range(1, T):
-            t = (tpi + o) % T
-            send(ps.at[t, c, h], pr.at[o, c, h], p_snd.at[c, h, o], p_rcv.at[c, h, o], tp=t).wait()
+            partial(h, c, o, (tpi + o) % T).wait_recv()
             total += pr[o, c, h].astype(F32)
         eo[c, h] = total.astype(BF16)
         for j in range(1, EPG):
-            p = partner(i, j, EPG)
-            send(
-                eo.at[c, h, slots(p)], ret.at[c, h, slots(i)], r_snd.at[c, h, p], r_rcv.at[c, h, i], fs=g * EPG + p
-            ).start()
+            return_to(h, c, partner(i, j, EPG), i).start()
         ret[c, h, slots(i), :] = eo[c, h, slots(i), :]
+
+    def result_to(h, c, q):
+        return send(ms.at[c, h], fin.at[c, q], f_snd.at[c, h], f_rcv.at[c, q], fs=h * EPG + i)
 
     def mix(c, h, last):
         for j in range(1, EPG):
-            p = (i + j) % EPG
-            send(
-                eo.at[c, h, slots(p)], ret.at[c, h, slots(p)], r_snd.at[c, h, p], r_rcv.at[c, h, p], fs=g * EPG + p
-            ).wait()
+            p = partner(i, j, EPG)
+            return_to(h, c, p, p).wait_recv()
         cols = i1r[h].T[:Rg]
         outs = ret[c, h]
         both = (cols[:, 2:3] * dot(sel[h, 0], outs) + cols[:, 3:4] * dot(sel[h, 1], outs)).astype(BF16)
@@ -275,23 +295,36 @@
             fin[c, g] = both
         else:
             ms[c, h] = both
-            send(ms.at[c, h], fin.at[c, g], f_snd.at[c, h], f_rcv.at[c, g], fs=h * EPG + i).start()
-
-    steps = [(c, (g + 1 + k) % G, k == G - 1) for k in range(G) for c in range(C)]
-    for s in range(len(steps) + 3):
-        if s < len(steps):
-            sum_units(*steps[s][:2])
-        if 1 <= s <= len(steps):
-            hand_back(*steps[s - 1][:2])
-        if s >= 3:
-            mix(*steps[s - 3])
+            result_to(h, c, g).start()
+
+    first = (me * T) // n
+    for k in range(T):
+        t = (first + k) % T
+        wait_weights(2, new_down, t * (n // T), n // T)
+        if k == T - 1:
+            stores[2].start()
+        for h in (*others, g):
+            for c in range(C):
+                sum_units(t, (t - tpi + T) % T, c, h)
+
+        @pl.when(t == tpi)
+        def _():
+            for h in (*others, g):
+                for c in range(C):
+                    hand_back(c, h)
+            for h in others:
+                for c in range(C):
+                    mix(c, h, False)
+
+    for c in range(C):
+        mix(c, g, True)
 
     for c in range(C):
         total = 0.0
         for k in (G - 1, *range(G - 1)):
             q = (g + 1 + k) % G
             if k < G - 1:
-                send(ms.at[c, q], fin.at[c, q], f_snd.at[c, q], f_rcv.at[c, q], fs=q * EPG + i).wait()
+                result_to(q, c, q).wait_recv()
             total += dot(place[q], fin[c, q])
         mixed[:, c * Dc : (c + 1) * Dc] = total.astype(BF16)
         stores.append(
@@ -302,6 +335,31 @@
         stores[-1].start()
     for store in stores:
         store.wait()
+
+    def drain(k, c):
+        p = (me + k) % n
+        for m, dst in enumerate((new_gate, new_up, new_down)):
+            weights_from(m, dst, p).wait_send()
+        return c
+
+    lax.fori_loop(1, n, drain, 0)
+    for h in (*others, g):
+        for o in range(1, T):
+            send(x.at[tpi, h], x.at[tpi, h], tp_snd.at[h, o], tp_rcv.at[h, o], tp=(tpi + o) % T).wait_send()
+        for j in range(1, EPG):
+            p = partner(i, j, EPG)
+            send(
+                s2s.at[h, slots(p)], x.at[tpi, h, slots(p)], s2_snd.at[h, p], s2_rcv.at[h, p], fs=g * EPG + p
+            ).wait_send()
+        for c in range(C):
+            for o in range(1, T):
+                partial(h, c, o, (tpi + o) % T).wait_send()
+            for j in range(1, EPG):
+                p = partner(i, j, EPG)
+                return_to(h, c, p, p).wait_send()
+    for h in others:
+        for c in range(C):
+            result_to(h, c, h).wait_send()
 
 
 def hand_over(count, *refs):

time: 150 us -> 140 us (0.933)
  the two profiles are of different devices: /device:TPU:0 before, /device:TPU:1 now
where the time goes in v2:
time: 140 us
  Pallas kernels  139 us (99%)
    pallas_call x1, Pallas kernels, local(): pl.pallas_call(functools.partial(kernel, n, T), out_shape=shapes, in_spec...  136 us
    pallas_call x1, Pallas kernels, local(): pl.pallas_call(functools.partial(hand_over, parts), out_shape=shapes, in_...  3.58 us

profile of v2, /device:TPU:1, one launch (start us, length us, event | category | flops | bytes accessed | tf_op | source)
XLA Modules:
  0.0 140.3 jit_solution(1423073837126448032)
XLA Ops:
  0.6 135.9 %shard_map.111 = (bf16[2048,256]{1,0:T(8,128)(2,1)}, bf16[2048,256]{1,0:T(8,128)(2,1)}, bf16[2048,256]{1,0:T(8,128)(2,1)}, bf16[512,1024]{1,0:T(8,128)(2,1)}) custom-call(s32[2,512]{1,0:T(2,128)} %bitcast.7, f32[1,128]{1,0:T(1,128)} %bitcast.10, f32[1,512]{1,0:T(1,128)} %bitcast.9, f32[2,512]{1,0:T(2,128)} %bitcast.8, bf16[512,2048]{1,0:T(8,128)(2,1)} %tokens_in.1, ...), custom_call_target="tpu_custom_call" | custom-call | tf_op jit(solution)/shard_map/pallas_call | solution.py:398
  136.6 3.6 %shard_map.112 = (bf16[2048,256]{1,0:T(8,128)(2,1)}, bf16[2048,256]{1,0:T(8,128)(2,1)}, bf16[2048,256]{1,0:T(8,128)(2,1)}, bf16[512,1024]{1,0:T(8,128)(2,1)}) custom-call(bf16[2048,256]{1,0:T(8,128)(2,1)} %get-tuple-element.12.refs_0_, bf16[2048,256]{1,0:T(8,128)(2,1)} %get-tuple-element.13.refs_1_, bf16[2048,256]{1,0:T(8,128)(2,1)} %get-tuple-element.14.refs_2_, ...), custom_call_target="tpu_custom_call" | custom-call | tf_op jit(solution)/shard_map/pallas_call | solution.py:446

commit v3 on v2

--- a/solution.py
+++ b/solution.py
@@ -8,11 +8,13 @@
 from jax.sharding import PartitionSpec as P
 
 EPG = 8
+SIDES = 2
 TOP = 2
 EPSILON = 1e-06
 MESH = pl.DeviceIdType.MESH
 F32, BF16 = jnp.float32, jnp.bfloat16
 CHUNKS = 4
+FAR_AFTER = 1
 VMEM_LIMIT = 62 * 1024 * 1024
 
 
@@ -56,6 +58,23 @@
     S = EPG * cap
     W = i1s.shape[2]
     C, Dc = ps.shape[1], ps.shape[4]
+    half = EPG // SIDES
+    lane, side = i % half, i // half
+    others = [(g + 1 + k) % G for k in range(G - 1)]
+
+    def side_for(q, h):
+        return (h - q + G) // G
+
+    def relays(h):
+        return side == side_for(g, h)
+
+    def outside(h):
+        return (SIDES * h) // G
+
+    def origins(h):
+        return [(outside(h) + k) % SIDES for k in range(SIDES)]
+
+    outer = side == outside(g)
 
     barrier = pltpu.get_barrier_semaphore()
 
@@ -94,27 +113,21 @@
         loads[1 + m].wait()
         lax.fori_loop(0, n, cast, 0)
 
+    per_part = n // T
+
+    def arrival(m, p):
+        return w_rcv.at[m + p // per_part if m == 2 else m]
+
     def send_weights(m, dst, order):
         for j in order:
             p = partner(me, j, n)
-            send(wb.at[m, p], dst.at[block(me)], w_snd.at[m, p], w_rcv.at[m, me], fs=p).start()
+            send(wb.at[m, p], dst.at[block(me)], w_snd.at[m], arrival(m, me), fs=p).start()
 
     near, far = range(1, EPG), range(EPG, n)
 
-    def weights_from(m, dst, p):
-        return send(wb.at[m, p], dst.at[block(p)], w_snd.at[m, p], w_rcv.at[m, p], fs=p)
-
-    def wait_weights(m, dst, first, count):
-        def body(k, c):
-            p = first + k
-
-            @pl.when(p != me)
-            def _():
-                weights_from(m, dst, p).wait_recv()
-
-            return c
-
-        lax.fori_loop(0, count, body, 0)
+    def blocks(m, dst, p, count):
+        rows = dst.at[pl.ds(0, count * K)]
+        return send(rows, rows, w_snd.at[m], arrival(m, p), fs=p)
 
     id0, id1 = ids[0:1, :].astype(F32), ids[1:2, :].astype(F32)
     gap = logit[0:1, :] - logit[1:2, :]
@@ -148,115 +161,160 @@
     loads[0].wait()
     lax.fori_loop(0, R // step, norm, 0)
 
-    for k in range(G):
-        q = (g + 1 + k) % G
+    def choose(q):
         pick = jnp.where((index_grid((W, R), 0) == pos) & (gid == q.astype(F32)), 1.0, 0.0)
         info_q = dot(table, pick, ((1,), (1,)), precision=lax.Precision.HIGHEST)
-        rows_q = dot(pick[:Rg].astype(BF16), normed[...]).astype(BF16)
-        if k == G - 1:
-            s1r[g] = rows_q
-            i1r[g] = info_q
-        else:
-            s1s[q] = rows_q
-            i1s[q] = info_q
-
-    cast_weights(0, w_gate, True)
+        return dot(pick[:Rg].astype(BF16), normed[...]).astype(BF16), info_q
+
+    for q in others:
+        s1s[q], i1s[q] = choose(q)
     pl.semaphore_wait(barrier, n - 1 + T - 1)
 
-    for k in range(G - 1):
-        q = (g + 1 + k) % G
-        send(i1s.at[q], i1r.at[g], i1_snd.at[q], i1_rcv.at[g], fs=q * EPG + i).start()
-        send(s1s.at[q], s1r.at[g], s1_snd.at[q], s1_rcv.at[g], fs=q * EPG + i).start()
-
-    def dispatch(h):
-        slot_q = i1r[h]
+    def rows_to(q):
+        return [
+            send(a.at[q], b.at[g, side], snd.at[q], rcv.at[g, side], fs=q * EPG + half * side_for(q, g) + lane)
+            for a, b, snd, rcv in ((i1s, i1r, i1_snd, i1_rcv), (s1s, s1r, s1_snd, s1_rcv))
+        ]
+
+    def rows_from(h, k):
+        return [
+            send(a.at[h], b.at[h, k], snd.at[h], rcv.at[h, k], fs=h * EPG)
+            for a, b, snd, rcv in ((i1s, i1r, i1_snd, i1_rcv), (s1s, s1r, s1_snd, s1_rcv))
+        ]
+
+    def slots_to(h, k, origin, p):
+        return send(
+            s2s.at[h, k, slots(p)], x.at[tpi, h, slots(origin)], s2_snd.at[h, k], s2_rcv.at[h, origin // half],
+            fs=g * EPG + p,
+        )
+
+    def dispatch(h, k, origin):
+        slot_q = i1r[h, k]
         grid = index_grid((S, Rg), 0)
         spread = (grid == slot_q[0:1, :Rg]) | (grid == slot_q[1:2, :Rg])
-        s2s[h] = dot(jnp.where(spread, 1.0, 0.0).astype(BF16), s1r[h]).astype(BF16)
+        s2s[h, k] = dot(jnp.where(spread, 1.0, 0.0).astype(BF16), s1r[h, k]).astype(BF16)
         for j in range(1, EPG):
-            p = partner(i, j, EPG)
-            send(
-                s2s.at[h, slots(p)], x.at[tpi, h, slots(i)], s2_snd.at[h, p], s2_rcv.at[h, i], fs=g * EPG + p
-            ).start()
-        x[tpi, h, slots(i), :] = s2s[h, slots(i), :]
-
-    dispatch(g)
+            slots_to(h, k, origin, partner(i, j, EPG)).start()
+        x[tpi, h, slots(origin), :] = s2s[h, k, slots(i), :]
+
+    def selection(h, k):
+        cols = i1r[h, k].T[:Rg]
+        grid = index_grid((Rg, S), 1)
+        for c in range(TOP):
+            sel[h, k, c] = jnp.where(grid == cols[:, c : c + 1], 1.0, 0.0).astype(BF16)
+
+    for q in others:
+        for copy in rows_to(q):
+            copy.start()
+    s1r[g, 0], i1r[g, 0] = choose(g)
+    dispatch(g, 0, i)
+    cast_weights(0, w_gate, True)
+    send_weights(0, new_gate, near)
+    cast_weights(1, w_up, True)
+    send_weights(1, new_up, near)
     send_weights(0, new_gate, far)
-    cast_weights(1, w_up, True)
     send_weights(1, new_up, far)
-    send_weights(0, new_gate, near)
-    send_weights(1, new_up, near)
     cast_weights(2, w_down, False)
     for m, dst in enumerate((new_gate, new_up, new_down)):
         dst[block(me), :] = wb[m, me]
 
-    for k in range(G - 1):
-        h = (g + 1 + k) % G
-        send(i1s.at[h], i1r.at[h], i1_snd.at[h], i1_rcv.at[h], fs=h * EPG + i).wait()
-        send(s1s.at[h], s1r.at[h], s1_snd.at[h], s1_rcv.at[h], fs=h * EPG + i).wait()
-        dispatch(h)
+    for h in others:
+
+        @pl.when(relays(h))
+        def _():
+            for k in origins(h):
+                for copy in rows_from(h, k):
+                    copy.wait_recv()
+                dispatch(h, k, k * half + lane)
+
     send_weights(2, new_down, near)
-    send_weights(2, new_down, far)
-
-    for k in range(G):
-        h = (g + 1 + k) % G
-        cols = i1r[h].T[:Rg]
-        grid = index_grid((Rg, S), 1)
-        for c in range(TOP):
-            sel[h, c] = jnp.where(grid == cols[:, c : c + 1], 1.0, 0.0).astype(BF16)
+
+    @pl.when(jnp.logical_not(outer))
+    def _():
+        send_weights(2, new_down, [b + j for b in range(EPG, n, EPG) for j in (*range(half, EPG), *range(half))])
+
+
+    for h in others:
+
+        @pl.when(relays(h))
+        def _():
+            for k in range(SIDES):
+                selection(h, k)
+
         grid = index_grid((R, Rg), 1)
         here = (grid == info_t[:, 5:6]) & (info_t[:, 4:5] == h.astype(F32))
         place[h] = jnp.where(here, 1.0, 0.0).astype(BF16)
-
-    def exchange(h):
-        for j in range(1, EPG):
-            p = partner(i, j, EPG)
-            send(
-                s2s.at[h, slots(p)], x.at[tpi, h, slots(p)], s2_snd.at[h, p], s2_rcv.at[h, p], fs=g * EPG + p
-            ).wait_recv()
+    selection(g, 0)
+    grid = index_grid((R, Rg), 1)
+    here = (grid == info_t[:, 5:6]) & (info_t[:, 4:5] == g.astype(F32))
+    place[g] = jnp.where(here, 1.0, 0.0).astype(BF16)
+
+    part = half * cap
+
+    def portion(k):
+        return pl.ds(pl.multiple_of(k * part, part), part)
+
+    def shared(t, h, k, o):
+        return send(
+            x.at[t, h, portion(k)], x.at[t, h, portion(k)], tp_snd.at[h, k, o - 1], tp_rcv.at[h, k, o - 1],
+            tp=(tpi + o) % T,
+        )
+
+    def take(ref, snd, rcv, full, count):
+        for missing in (0, 1):
+
+            @pl.when(full if missing == 0 else jnp.logical_not(full))
+            def _():
+                rows = ref.at[pl.ds(0, (count - missing) * cap)]
+                send(rows, rows, snd, rcv, fs=me).wait_recv()
+
+    def exchange(h, k, whole):
+        take(x.at[tpi, h], s2_snd.at[h, k], s2_rcv.at[h, k], whole, half)
         for o in range(1, T):
-            send(x.at[tpi, h], x.at[tpi, h], tp_snd.at[h, o], tp_rcv.at[h, o], tp=(tpi + o) % T).start()
-
-    def exchanged(h):
+            shared(tpi, h, k, o).start()
+
+    def exchanged(h, k):
         for o in range(1, T):
-            t = (tpi + T - o) % T
-            send(x.at[t, h], x.at[t, h], tp_snd.at[h, o], tp_rcv.at[h, o], tp=(tpi + o) % T).wait_recv()
-
-    tile = min(S, 256)
-
-    def apply_experts(h):
-        def expert(b, c):
-            rows = pl.ds(pl.multiple_of(b * tile, tile), tile)
-            gate_pre = up_pre = 0.0
-            for t in range(T):
-                part = x[t, h, rows, :]
-                gate_pre += dot(part, new_gate[t * Dt : (t + 1) * Dt, :])
-                up_pre += dot(part, new_up[t * Dt : (t + 1) * Dt, :])
-            hid[h, rows, :] = (gate_pre / (1.0 + jnp.exp(-gate_pre)) * up_pre).astype(BF16)
-            return c
-
-        lax.fori_loop(0, S // tile, expert, 0)
+            shared((tpi + T - o) % T, h, k, o).wait_recv()
+
+    def apply_experts(h, k):
+        rows = portion(k)
+        gate_pre = up_pre = 0.0
+        for t in range(T):
+            piece = x[t, h, rows, :]
+            gate_pre += dot(piece, new_gate[t * Dt : (t + 1) * Dt, :])
+            up_pre += dot(piece, new_up[t * Dt : (t + 1) * Dt, :])
+        hid[h, rows, :] = (gate_pre / (1.0 + jnp.exp(-gate_pre)) * up_pre).astype(BF16)
 
     stores = [
         pltpu.make_async_copy(src, dst, out_sem.at[k])
         for k, (src, dst) in enumerate(((new_gate, gate_out), (new_up, up_out), (new_down, down_out)))
     ]
-    others = [(g + 1 + k) % G for k in range(G - 1)]
-    exchange(g)
-    for h in others:
-        exchange(h)
-    wait_weights(0, new_gate, 0, n)
+    for k in range(SIDES):
+        exchange(g, k, side != k)
+    blocks(0, new_gate, me, n - 1).wait_recv()
     stores[0].start()
-    wait_weights(1, new_up, 0, n)
+    for at in range(SIDES):
+        for h in others:
+            exchange(h, origins(h)[at], jnp.logical_not(relays(h)))
+        if at == FAR_AFTER:
+
+            @pl.when(outer)
+            def _():
+                send_weights(2, new_down, far)
+
+    blocks(1, new_up, me, n - 1).wait_recv()
     stores[1].start()
-    exchanged(g)
-    apply_experts(g)
-    for h in others:
-        exchanged(h)
-        apply_experts(h)
+    for k in range(SIDES):
+        exchanged(g, k)
+        apply_experts(g, k)
+    for at in range(SIDES):
+        for h in others:
+            exchanged(h, origins(h)[at])
+            apply_experts(h, origins(h)[at])
 
     def partial(h, c, o, t):
-        return send(ps.at[o, c, h], pr.at[o, c, h], p_snd.at[c, h, o], p_rcv.at[c, h, o], tp=t)
+        return send(ps.at[o, c, h], pr.at[o, c, h], p_snd.at[0], p_rcv.at[c, h, o - 1], tp=t)
 
     def sum_units(t, o, c, h):
         rows = pl.ds(pl.multiple_of(t * Dt + c * Dc, Dc), Dc)
@@ -266,65 +324,103 @@
         def _():
             partial(h, c, o, t).start()
 
-    def return_to(h, c, p, q):
+    def return_to(h, c, k, origin, p, q):
         return send(
-            eo.at[c, h, slots(p)], ret.at[c, h, slots(q)], r_snd.at[c, h, p], r_rcv.at[c, h, q], fs=g * EPG + p
+            eo.at[c, h, slots(origin)], ret.at[c, h, k, slots(q)], r_snd.at[h], r_rcv.at[c, h, k],
+            fs=g * EPG + p,
         )
 
-    def hand_back(c, h):
+    def total_units(c, h):
         total = ps[0, c, h].astype(F32)
         for o in range(1, T):
             partial(h, c, o, (tpi + o) % T).wait_recv()
             total += pr[o, c, h].astype(F32)
         eo[c, h] = total.astype(BF16)
-        for j in range(1, EPG):
-            return_to(h, c, partner(i, j, EPG), i).start()
-        ret[c, h, slots(i), :] = eo[c, h, slots(i), :]
-
-    def result_to(h, c, q):
-        return send(ms.at[c, h], fin.at[c, q], f_snd.at[c, h], f_rcv.at[c, q], fs=h * EPG + i)
-
-    def mix(c, h, last):
+
+    def hand_back_other(c, h):
+        total_units(c, h)
+        at = half * side_for(g, h)
+        for k in range(SIDES):
+
+            @pl.when(relays(h))
+            def _():
+                ret[c, h, k, slots(i), :] = eo[c, h, slots(k * half + lane), :]
+
+            @pl.when(jnp.logical_not(relays(h)))
+            def _():
+                return_to(h, c, k, k * half + lane, at + lane, i).start()
+
+            for j in range(1, half):
+                l = partner(lane, j, half)
+                return_to(h, c, k, k * half + l, at + l, i).start()
+
+    def hand_back_own(c):
+        total_units(c, g)
         for j in range(1, EPG):
             p = partner(i, j, EPG)
-            return_to(h, c, p, p).wait_recv()
-        cols = i1r[h].T[:Rg]
-        outs = ret[c, h]
-        both = (cols[:, 2:3] * dot(sel[h, 0], outs) + cols[:, 3:4] * dot(sel[h, 1], outs)).astype(BF16)
-        if last:
-            fin[c, g] = both
-        else:
-            ms[c, h] = both
-            result_to(h, c, g).start()
-
-    first = (me * T) // n
+            return_to(g, c, 0, p, p, i).start()
+        ret[c, g, 0, slots(i), :] = eo[c, g, slots(i), :]
+
+    def result_to(h, c, k, q):
+        return send(
+            ms.at[c, h, k], fin.at[c, q], f_snd.at[h, k], f_rcv.at[c, q], fs=h * EPG + k * half + lane
+        )
+
+    def mix(c, h, k):
+        rows = ret.at[c, h, k, pl.ds(0, (EPG - 1) * cap)]
+        send(rows, rows, r_snd.at[h], r_rcv.at[c, h, k], fs=me).wait_recv()
+        cols = i1r[h, k].T[:Rg]
+        outs = ret[c, h, k]
+        return (cols[:, 2:3] * dot(sel[h, k, 0], outs) + cols[:, 3:4] * dot(sel[h, k, 1], outs)).astype(BF16)
+
+    def mix_other(c, h):
+        @pl.when(relays(h))
+        def _():
+            for k in range(SIDES):
+                ms[c, h, k] = mix(c, h, k)
+                result_to(h, c, k, g).start()
+
+    first = me // per_part
     for k in range(T):
         t = (first + k) % T
-        wait_weights(2, new_down, t * (n // T), n // T)
+        if k == 0:
+            blocks(2, new_down, me, per_part - 1).wait_recv()
+        else:
+            blocks(2, new_down, t * per_part, per_part).wait_recv()
         if k == T - 1:
             stores[2].start()
-        for h in (*others, g):
+        for h in others:
             for c in range(C):
                 sum_units(t, (t - tpi + T) % T, c, h)
 
         @pl.when(t == tpi)
         def _():
-            for h in (*others, g):
-                for c in range(C):
-                    hand_back(c, h)
             for h in others:
                 for c in range(C):
-                    mix(c, h, False)
+                    hand_back_other(c, h)
+
+        for c in range(C):
+            sum_units(t, (t - tpi + T) % T, c, g)
+
+        @pl.when(t == tpi)
+        def _():
+            for c in range(C):
+                hand_back_own(c)
+
+
+    for h in others:
+        for c in range(C):
+            mix_other(c, h)
 
     for c in range(C):
-        mix(c, g, True)
+        fin[c, g] = mix(c, g, 0)
 
     for c in range(C):
         total = 0.0
         for k in (G - 1, *range(G - 1)):
             q = (g + 1 + k) % G
             if k < G - 1:
-                result_to(q, c, q).wait_recv()
+                result_to(q, c, 0, q).wait_recv()
             total += dot(place[q], fin[c, q])
         mixed[:, c * Dc : (c + 1) * Dc] = total.astype(BF16)
         stores.append(
@@ -336,30 +432,34 @@
     for store in stores:
         store.wait()
 
-    def drain(k, c):
-        p = (me + k) % n
-        for m, dst in enumerate((new_gate, new_up, new_down)):
-            weights_from(m, dst, p).wait_send()
-        return c
-
-    lax.fori_loop(1, n, drain, 0)
+    def drain(ref, sem):
+        send(ref, ref, sem, sem, fs=me).wait_send()
+
+    for m in range(3):
+        drain(wb.at[m, pl.ds(0, n - 1)], w_snd.at[m])
+    sent = pl.ds(0, (EPG - 1) * cap)
+    drain(s2s.at[g, 0, sent], s2_snd.at[g, 0])
+    drain(eo.at[pl.ds(0, C), g, sent], r_snd.at[g])
+    if T > 1:
+        drain(ps.at[pl.ds(1, T - 1)], p_snd.at[0])
     for h in (*others, g):
-        for o in range(1, T):
-            send(x.at[tpi, h], x.at[tpi, h], tp_snd.at[h, o], tp_rcv.at[h, o], tp=(tpi + o) % T).wait_send()
-        for j in range(1, EPG):
-            p = partner(i, j, EPG)
-            send(
-                s2s.at[h, slots(p)], x.at[tpi, h, slots(p)], s2_snd.at[h, p], s2_rcv.at[h, p], fs=g * EPG + p
-            ).wait_send()
-        for c in range(C):
+        for k in range(SIDES):
             for o in range(1, T):
-                partial(h, c, o, (tpi + o) % T).wait_send()
-            for j in range(1, EPG):
-                p = partner(i, j, EPG)
-                return_to(h, c, p, p).wait_send()
+                shared(tpi, h, k, o).wait_send()
     for h in others:
-        for c in range(C):
-            result_to(h, c, h).wait_send()
+        for copy in rows_to(h):
+            copy.wait_send()
+
+        @pl.when(relays(h))
+        def _():
+            drain(eo.at[pl.ds(0, C), h, pl.ds(0, (EPG - SIDES) * cap)], r_snd.at[h])
+            for k in range(SIDES):
+                drain(s2s.at[h, k, sent], s2_snd.at[h, k])
+                drain(ms.at[pl.ds(0, C), h, k], f_snd.at[h, k])
+
+        @pl.when(jnp.logical_not(relays(h)))
+        def _():
+            drain(eo.at[pl.ds(0, C), h], r_snd.at[h])
 
 
 def hand_over(count, *refs):
@@ -414,26 +514,26 @@
             pltpu.VMEM((R, 8), F32),
             pltpu.VMEM((G, Rg, Dt), BF16),
             pltpu.VMEM((G, 8, W), F32),
-            pltpu.VMEM((G, Rg, Dt), BF16),
-            pltpu.VMEM((G, 8, W), F32),
-            pltpu.VMEM((G, S, Dt), BF16),
+            pltpu.VMEM((G, SIDES, Rg, Dt), BF16),
+            pltpu.VMEM((G, SIDES, 8, W), F32),
+            pltpu.VMEM((G, SIDES, S, Dt), BF16),
             pltpu.VMEM((T, G, S, Dt), BF16),
-            pltpu.VMEM((G, TOP, Rg, S), BF16),
+            pltpu.VMEM((G, SIDES, TOP, Rg, S), BF16),
             pltpu.VMEM((G, R, Rg), BF16),
             pltpu.VMEM((G, S, F), BF16),
             pltpu.VMEM((T, C, G, S, Dc), BF16),
             pltpu.VMEM((T, C, G, S, Dc), BF16),
             pltpu.VMEM((C, G, S, Dc), BF16),
-            pltpu.VMEM((C, G, S, Dc), BF16),
-            pltpu.VMEM((C, G, Rg, Dc), BF16),
+            pltpu.VMEM((C, G, SIDES, S, Dc), BF16),
+            pltpu.VMEM((C, G, SIDES, Rg, Dc), BF16),
             pltpu.VMEM((C, G, Rg, Dc), BF16),
             sem((4,)), sem((3 + C,)),
-            sem((3, n)), sem((3, n)),
-            sem((G,)), sem((G,)), sem((G,)), sem((G,)),
-            sem((G, EPG)), sem((G, EPG)),
-            sem((G, T)), sem((G, T)), sem((C, G, T)), sem((C, G, T)),
-            sem((C, G, EPG)), sem((C, G, EPG)),
-            sem((C, G)), sem((C, G)),
+            sem((3,)), sem((2 + T,)),
+            sem((G,)), sem((G, SIDES)), sem((G,)), sem((G, SIDES)),
+            sem((G, SIDES)), sem((G, SIDES)),
+            sem((G, SIDES, max(T - 1, 1))), sem((G, SIDES, max(T - 1, 1))), sem((1,)), sem((C, G, max(T - 1, 1))),
+            sem((G,)), sem((C, G, SIDES)),
+            sem((G, SIDES)), sem((C, G)),
         ],
         compiler_params=pltpu.CompilerParams(
             collective_id=0, has_side_effects=True, vmem_limit_bytes=VMEM_LIMIT

time: 140 us -> 131 us (0.936)
  the two profiles are of different devices: /device:TPU:1 before, /device:TPU:0 now
where the time goes in v3:
time: 131 us; the launch traced here: 130 us
  Pallas kernels  129 us (98%)
    pallas_call x1, Pallas kernels, local(): pl.pallas_call(functools.partial(kernel, n, T), out_shape=shapes, in_spec...  126 us
    pallas_call x1, Pallas kernels, local(): pl.pallas_call(functools.partial(hand_over, parts), out_shape=shapes, in_...  3.58 us

profile of v3, /device:TPU:0, one launch (start us, length us, event | category | flops | bytes accessed | tf_op | source)
XLA Modules:
  0.0 130.0 jit_solution(801842720465799286)
XLA Ops:
  0.6 125.6 %shard_map.111 = (bf16[2048,256]{1,0:T(8,128)(2,1)}, bf16[2048,256]{1,0:T(8,128)(2,1)}, bf16[2048,256]{1,0:T(8,128)(2,1)}, bf16[512,1024]{1,0:T(8,128)(2,1)}) custom-call(s32[2,512]{1,0:T(2,128)} %bitcast.7, f32[1,128]{1,0:T(1,128)} %bitcast.10, f32[1,512]{1,0:T(1,128)} %bitcast.9, f32[2,512]{1,0:T(2,128)} %bitcast.8, bf16[512,2048]{1,0:T(8,128)(2,1)} %tokens_in.1, ...), custom_call_target="tpu_custom_call" | custom-call | tf_op jit(solution)/shard_map/pallas_call | solution.py:498
  126.2 3.6 %shard_map.112 = (bf16[2048,256]{1,0:T(8,128)(2,1)}, bf16[2048,256]{1,0:T(8,128)(2,1)}, bf16[2048,256]{1,0:T(8,128)(2,1)}, bf16[512,1024]{1,0:T(8,128)(2,1)}) custom-call(bf16[2048,256]{1,0:T(8,128)(2,1)} %get-tuple-element.12.refs_0_, bf16[2048,256]{1,0:T(8,128)(2,1)} %get-tuple-element.13.refs_1_, bf16[2048,256]{1,0:T(8,128)(2,1)} %get-tuple-element.14.refs_2_, ...), custom_call_target="tpu_custom_call" | custom-call | tf_op jit(solution)/shard_map/pallas_call | solution.py:546

commit v4 on v3

--- a/solution.py
+++ b/solution.py
@@ -44,8 +44,8 @@
 
 
 def kernel(
-    n, T, ids, gain, prob, logit, tokens_in, gate_in, up_in, down_in, gate_out, up_out, down_out, mixed_out,
-    tokens, w_gate, w_up, w_down, new_gate, new_up, new_down, mixed,
+    n, T, ids_in, gain_in, prob_in, logit_in, tokens_in, gate_in, up_in, down_in, gate_out, up_out, down_out, mixed_out,
+    ids, gain, prob, logit, tokens, w_gate, w_up, w_down, new_gate, new_up, new_down, mixed,
     wb, normed, info_t, s1s, i1s, s1r, i1r, s2s, x, sel, place, hid, ps, pr, eo, ret, ms, fin,
     in_sem, out_sem, w_snd, w_rcv, s1_snd, s1_rcv, i1_snd, i1_rcv, s2_snd, s2_rcv, tp_snd, tp_rcv,
     p_snd, p_rcv, r_snd, r_rcv, f_snd, f_rcv,
@@ -78,6 +78,18 @@
 
     barrier = pltpu.get_barrier_semaphore()
 
+    loads = [
+        pltpu.make_async_copy(src, dst, in_sem.at[k])
+        for k, (src, dst) in enumerate(
+            (
+                (gate_in, w_gate), (up_in, w_up), (down_in, w_down), (tokens_in, tokens),
+                (ids_in, ids), (logit_in, logit), (prob_in, prob), (gain_in, gain),
+            )
+        )
+    ]
+    for k in (4, 5, 6, 3, 7, 0, 1, 2):
+        loads[k].start()
+
     def greet(k, c):
         pl.semaphore_signal(barrier, inc=1, device_id={"fs": (me + k) % n}, device_id_type=MESH)
         return c
@@ -86,31 +98,25 @@
     for o in range(1, T):
         pl.semaphore_signal(barrier, inc=1, device_id={"tp": (tpi + o) % T}, device_id_type=MESH)
 
-    loads = [
-        pltpu.make_async_copy(src, dst, in_sem.at[k])
-        for k, (src, dst) in enumerate(
-            ((tokens_in, tokens), (gate_in, w_gate), (up_in, w_up), (down_in, w_down))
-        )
-    ]
-    for load in loads:
-        load.start()
-
     def block(p):
         return pl.ds(pl.multiple_of(p * K, K), K)
 
     def slots(p):
         return pl.ds(pl.multiple_of(p * cap, cap), cap)
 
-    diagonal = index_grid((K, K), 0) == index_grid((K, K), 1)
-    gains = jnp.sum(jnp.where(diagonal, gain[...], 0.0), axis=1, keepdims=True)
+    def spread_gain():
+        diagonal = index_grid((K, K), 0) == index_grid((K, K), 1)
+        return jnp.sum(jnp.where(diagonal, gain[...], 0.0), axis=1, keepdims=True)
 
     def cast_weights(m, src, scaled):
+        gains = spread_gain() if scaled else None
+
         def cast(p, c):
             v = src[p]
             wb[m, p] = (v * gains if scaled else v).astype(BF16)
             return c
 
-        loads[1 + m].wait()
+        loads[m].wait()
         lax.fori_loop(0, n, cast, 0)
 
     per_part = n // T
@@ -129,6 +135,8 @@
         rows = dst.at[pl.ds(0, count * K)]
         return send(rows, rows, w_snd.at[m], arrival(m, p), fs=p)
 
+    for k in (4, 5, 6):
+        loads[k].wait()
     id0, id1 = ids[0:1, :].astype(F32), ids[1:2, :].astype(F32)
     gap = logit[0:1, :] - logit[1:2, :]
     gid = jnp.floor(id0 * (1.0 / EPG))
@@ -158,7 +166,7 @@
         normed[rows, :] = (part * scale).astype(BF16)
         return c
 
-    loads[0].wait()
+    loads[3].wait()
     lax.fori_loop(0, R // step, norm, 0)
 
     def choose(q):
@@ -207,6 +215,7 @@
         for copy in rows_to(q):
             copy.start()
     s1r[g, 0], i1r[g, 0] = choose(g)
+    loads[7].wait()
     dispatch(g, 0, i)
     cast_weights(0, w_gate, True)
     send_weights(0, new_gate, near)
@@ -414,13 +423,9 @@
 
     for c in range(C):
         fin[c, g] = mix(c, g, 0)
-
-    for c in range(C):
-        total = 0.0
-        for k in (G - 1, *range(G - 1)):
-            q = (g + 1 + k) % G
-            if k < G - 1:
-                result_to(q, c, 0, q).wait_recv()
+        total = dot(place[g], fin[c, g])
+        for q in others:
+            result_to(q, c, 0, q).wait_recv()
             total += dot(place[q], fin[c, q])
         mixed[:, c * Dc : (c + 1) * Dc] = total.astype(BF16)
         stores.append(
@@ -490,7 +495,6 @@
     S, W = EPG * cap, max(Rg, 128)
     Dc = min(Dt, max(Dt // CHUNKS, 128))
     C = Dt // Dc
-    vmem = pl.BlockSpec(memory_space=pltpu.VMEM)
     hbm = pl.BlockSpec(memory_space=pl.ANY)
     sem = pltpu.SemaphoreType.DMA
     weights = jax.ShapeDtypeStruct((D, F), BF16)
@@ -498,9 +502,13 @@
     results = pl.pallas_call(
         functools.partial(kernel, n, T),
         out_shape=shapes,
-        in_specs=[vmem] * 4 + [hbm] * 4,
+        in_specs=[hbm] * 8,
         out_specs=[hbm] * 4,
         scratch_shapes=[
+            pltpu.VMEM((TOP, R), jnp.int32),
+            pltpu.VMEM((1, D // n), F32),
+            pltpu.VMEM((1, R), F32),
+            pltpu.VMEM((TOP, R), F32),
             pltpu.VMEM((R, D), BF16),
             pltpu.VMEM(w_gate.shape, F32),
             pltpu.VMEM(w_up.shape, F32),
@@ -527,7 +535,7 @@
             pltpu.VMEM((C, G, SIDES, S, Dc), BF16),
             pltpu.VMEM((C, G, SIDES, Rg, Dc), BF16),
             pltpu.VMEM((C, G, Rg, Dc), BF16),
-            sem((4,)), sem((3 + C,)),
+            sem((8,)), sem((3 + C,)),
             sem((3,)), sem((2 + T,)),
             sem((G,)), sem((G, SIDES)), sem((G,)), sem((G, SIDES)),
             sem((G, SIDES)), sem((G, SIDES)),

time: 131 us -> 130 us (level)
  no operation moved by 1% of the time
where the time goes in v4:
time: 130 us; the launch traced here: 129 us
  Pallas kernels  128 us (98%)
    pallas_call x1, Pallas kernels, local(): pl.pallas_call(functools.partial(kernel, n, T), out_shape=shapes, in_spec...  125 us
    pallas_call x1, Pallas kernels, local(): pl.pallas_call(functools.partial(hand_over, parts), out_shape=shapes, in_...  3.58 us

profile of v4, /device:TPU:0, one launch (start us, length us, event | category | flops | bytes accessed | tf_op | source)
XLA Modules:
  0.0 129.3 jit_solution(4620467484682614300)
XLA Ops:
  0.6 124.9 %shard_map.111 = (bf16[2048,256]{1,0:T(8,128)(2,1)}, bf16[2048,256]{1,0:T(8,128)(2,1)}, bf16[2048,256]{1,0:T(8,128)(2,1)}, bf16[512,1024]{1,0:T(8,128)(2,1)}) custom-call(s32[2,512]{1,0:T(2,128)} %bitcast.7, f32[1,128]{1,0:T(1,128)} %bitcast.10, f32[1,512]{1,0:T(1,128)} %bitcast.9, f32[2,512]{1,0:T(2,128)} %bitcast.8, bf16[512,2048]{1,0:T(8,128)(2,1)} %tokens_in.1, ...), custom_call_target="tpu_custom_call" | custom-call | tf_op jit(solution)/shard_map/pallas_call | solution.py:502
  125.5 3.6 %shard_map.112 = (bf16[2048,256]{1,0:T(8,128)(2,1)}, bf16[2048,256]{1,0:T(8,128)(2,1)}, bf16[2048,256]{1,0:T(8,128)(2,1)}, bf16[512,1024]{1,0:T(8,128)(2,1)}) custom-call(bf16[2048,256]{1,0:T(8,128)(2,1)} %get-tuple-element.12.refs_0_, bf16[2048,256]{1,0:T(8,128)(2,1)} %get-tuple-element.13.refs_1_, bf16[2048,256]{1,0:T(8,128)(2,1)} %get-tuple-element.14.refs_2_, ...), custom_call_target="tpu_custom_call" | custom-call | tf_op jit(solution)/shard_map/pallas_call | solution.py:554

commit v5 on v4

--- a/solution.py
+++ b/solution.py
@@ -14,7 +14,7 @@
 MESH = pl.DeviceIdType.MESH
 F32, BF16 = jnp.float32, jnp.bfloat16
 CHUNKS = 4
-FAR_AFTER = 1
+STRIPS = 4
 VMEM_LIMIT = 62 * 1024 * 1024
 
 
@@ -78,17 +78,21 @@
 
     barrier = pltpu.get_barrier_semaphore()
 
+    step = min(R, 64)
+    strip = max(R // STRIPS, step)
+    strips = [pl.ds(k * strip, strip) for k in range(R // strip)]
     loads = [
         pltpu.make_async_copy(src, dst, in_sem.at[k])
         for k, (src, dst) in enumerate(
             (
-                (gate_in, w_gate), (up_in, w_up), (down_in, w_down), (tokens_in, tokens),
+                (gate_in, w_gate), (up_in, w_up), (down_in, w_down),
                 (ids_in, ids), (logit_in, logit), (prob_in, prob), (gain_in, gain),
+                *((tokens_in.at[rows], tokens.at[rows]) for rows in strips),
             )
         )
     ]
-    for k in (4, 5, 6, 3, 7, 0, 1, 2):
-        loads[k].start()
+    for load in loads[3:]:
+        load.start()
 
     def greet(k, c):
         pl.semaphore_signal(barrier, inc=1, device_id={"fs": (me + k) % n}, device_id_type=MESH)
@@ -135,8 +139,8 @@
         rows = dst.at[pl.ds(0, count * K)]
         return send(rows, rows, w_snd.at[m], arrival(m, p), fs=p)
 
-    for k in (4, 5, 6):
-        loads[k].wait()
+    for load in loads[3:6]:
+        load.wait()
     id0, id1 = ids[0:1, :].astype(F32), ids[1:2, :].astype(F32)
     gap = logit[0:1, :] - logit[1:2, :]
     gid = jnp.floor(id0 * (1.0 / EPG))
@@ -156,8 +160,6 @@
         table = jnp.where(line == at, value, table)
     info_t[...] = table.T
 
-    step = 64
-
     def norm(b, c):
         rows = pl.ds(pl.multiple_of(b * step, step), step)
         v = tokens[rows, :].astype(F32)
@@ -166,8 +168,12 @@
         normed[rows, :] = (part * scale).astype(BF16)
         return c
 
-    loads[3].wait()
-    lax.fori_loop(0, R // step, norm, 0)
+    for k, load in enumerate(loads[7:]):
+        load.wait()
+        if k == len(strips) - 1:
+            for late in loads[:3]:
+                late.start()
+        lax.fori_loop(k * strip // step, (k + 1) * strip // step, norm, 0)
 
     def choose(q):
         pick = jnp.where((index_grid((W, R), 0) == pos) & (gid == q.astype(F32)), 1.0, 0.0)
@@ -215,7 +221,7 @@
         for copy in rows_to(q):
             copy.start()
     s1r[g, 0], i1r[g, 0] = choose(g)
-    loads[7].wait()
+    loads[6].wait()
     dispatch(g, 0, i)
     cast_weights(0, w_gate, True)
     send_weights(0, new_gate, near)
@@ -306,11 +312,9 @@
     for at in range(SIDES):
         for h in others:
             exchange(h, origins(h)[at], jnp.logical_not(relays(h)))
-        if at == FAR_AFTER:
-
-            @pl.when(outer)
-            def _():
-                send_weights(2, new_down, far)
+        @pl.when(outer)
+        def _():
+            send_weights(2, new_down, [[EPG], range(EPG + 1, n)][at])
 
     blocks(1, new_up, me, n - 1).wait_recv()
     stores[1].start()
@@ -535,7 +539,7 @@
             pltpu.VMEM((C, G, SIDES, S, Dc), BF16),
             pltpu.VMEM((C, G, SIDES, Rg, Dc), BF16),
             pltpu.VMEM((C, G, Rg, Dc), BF16),
-            sem((8,)), sem((3 + C,)),
+            sem((7 + STRIPS,)), sem((3 + C,)),
             sem((3,)), sem((2 + T,)),
             sem((G,)), sem((G, SIDES)), sem((G,)), sem((G, SIDES)),
             sem((G, SIDES)), sem((G, SIDES)),

time: 130 us -> 128 us (0.985)
    pallas_call x1, Pallas kernels: 125 us -> 123 us  [local(): pl.pallas_call(functools.partial(kernel, n, T), out_shape=shapes, in_spec...]
where the time goes in v5:
time: 128 us
  Pallas kernels  127 us (99%)
    pallas_call x1, Pallas kernels, local(): pl.pallas_call(functools.partial(kernel, n, T), out_shape=shapes, in_spec...  123 us
    pallas_call x1, Pallas kernels, local(): pl.pallas_call(functools.partial(hand_over, parts), out_shape=shapes, in_...  3.58 us

profile of v5, /device:TPU:0, one launch (start us, length us, event | category | flops | bytes accessed | tf_op | source)
XLA Modules:
  0.0 127.6 jit_solution(12619306803943225726)
XLA Ops:
  0.6 123.2 %shard_map.111 = (bf16[2048,256]{1,0:T(8,128)(2,1)}, bf16[2048,256]{1,0:T(8,128)(2,1)}, bf16[2048,256]{1,0:T(8,128)(2,1)}, bf16[512,1024]{1,0:T(8,128)(2,1)}) custom-call(s32[2,512]{1,0:T(2,128)} %bitcast.7, f32[1,128]{1,0:T(1,128)} %bitcast.10, f32[1,512]{1,0:T(1,128)} %bitcast.9, f32[2,512]{1,0:T(2,128)} %bitcast.8, bf16[512,2048]{1,0:T(8,128)(2,1)} %tokens_in.1, ...), custom_call_target="tpu_custom_call" | custom-call | tf_op jit(solution)/shard_map/pallas_call | solution.py:506
  123.8 3.6 %shard_map.112 = (bf16[2048,256]{1,0:T(8,128)(2,1)}, bf16[2048,256]{1,0:T(8,128)(2,1)}, bf16[2048,256]{1,0:T(8,128)(2,1)}, bf16[512,1024]{1,0:T(8,128)(2,1)}) custom-call(bf16[2048,256]{1,0:T(8,128)(2,1)} %get-tuple-element.12.refs_0_, bf16[2048,256]{1,0:T(8,128)(2,1)} %get-tuple-element.13.refs_1_, bf16[2048,256]{1,0:T(8,128)(2,1)} %get-tuple-element.14.refs_2_, ...), custom_call_target="tpu_custom_call" | custom-call | tf_op jit(solution)/shard_map/pallas_call | solution.py:558

commit v6 on v5

--- a/solution.py
+++ b/solution.py
@@ -314,7 +314,7 @@
             exchange(h, origins(h)[at], jnp.logical_not(relays(h)))
         @pl.when(outer)
         def _():
-            send_weights(2, new_down, [[EPG], range(EPG + 1, n)][at])
+            send_weights(2, new_down, [range(EPG, EPG + 2), range(EPG + 2, n)][at])
 
     blocks(1, new_up, me, n - 1).wait_recv()
     stores[1].start()

time: 128 us -> 134 us (1.047); the launches traced: 128 us -> 132 us
  Pallas kernels: 127 us -> 131 us
    pallas_call x1, Pallas kernels: 123 us -> 128 us  [local(): pl.pallas_call(functools.partial(kernel, n, T), out_shape=shapes, in_spec...]
where the time goes in v6:
time: 134 us; the launch traced here: 132 us
  Pallas kernels  131 us (98%)
    pallas_call x1, Pallas kernels, local(): pl.pallas_call(functools.partial(kernel, n, T), out_shape=shapes, in_spec...  128 us
    pallas_call x1, Pallas kernels, local(): pl.pallas_call(functools.partial(hand_over, parts), out_shape=shapes, in_...  3.58 us

profile of v6, /device:TPU:0, one launch (start us, length us, event | category | flops | bytes accessed | tf_op | source)
XLA Modules:
  0.0 132.0 jit_solution(547153700424921310)
XLA Ops:
  0.6 127.6 %shard_map.111 = (bf16[2048,256]{1,0:T(8,128)(2,1)}, bf16[2048,256]{1,0:T(8,128)(2,1)}, bf16[2048,256]{1,0:T(8,128)(2,1)}, bf16[512,1024]{1,0:T(8,128)(2,1)}) custom-call(s32[2,512]{1,0:T(2,128)} %bitcast.7, f32[1,128]{1,0:T(1,128)} %bitcast.10, f32[1,512]{1,0:T(1,128)} %bitcast.9, f32[2,512]{1,0:T(2,128)} %bitcast.8, bf16[512,2048]{1,0:T(8,128)(2,1)} %tokens_in.1, ...), custom_call_target="tpu_custom_call" | custom-call | tf_op jit(solution)/shard_map/pallas_call | solution.py:506
  128.2 3.6 %shard_map.112 = (bf16[2048,256]{1,0:T(8,128)(2,1)}, bf16[2048,256]{1,0:T(8,128)(2,1)}, bf16[2048,256]{1,0:T(8,128)(2,1)}, bf16[512,1024]{1,0:T(8,128)(2,1)}) custom-call(bf16[2048,256]{1,0:T(8,128)(2,1)} %get-tuple-element.12.refs_0_, bf16[2048,256]{1,0:T(8,128)(2,1)} %get-tuple-element.13.refs_1_, bf16[2048,256]{1,0:T(8,128)(2,1)} %get-tuple-element.14.refs_2_, ...), custom_call_target="tpu_custom_call" | custom-call | tf_op jit(solution)/shard_map/pallas_call | solution.py:558
